TPU v7x, 256 devices: a 4x2x16 block of a 4x16x16 slice. The times are simulated.
256 devices in a mesh: grp: 2 (over y), ep: 32 (over z, core), tp: 4 (over x).
Axes of the slice: x: 4, y: 2, z: 16, core: 2. Of those that a mesh axis runs over, the one named last changes fastest.
The devices are a block of a 4x16x16 slice.
Arguments:
- queries: bfloat16 [8192, 2048], P(('grp', 'ep'), 'tp'), parts along dimension 0, may hold values from -6 to 6
- keys: bfloat16 [8192, 2048], P(('grp', 'ep'), 'tp'), parts along dimension 0, may hold values from -6 to 6
- values: bfloat16 [8192, 2048], P(('grp', 'ep'), 'tp'), parts along dimension 0, may hold values from -6 to 6
- stop_bias: bfloat16 [8192, 32], P(('grp', 'ep'), 'tp'), parts along dimension 0, may hold values from -20 to 0
- out_weight: bfloat16 [2048, 2048], P('tp'), may hold values from -0.125 to 0.125
- mix_gain: float32 [2048], replicated, may hold values from 0.1 to 1.9
- moe_input: bfloat16 [32768, 2048], P(('grp', 'ep', 'tp')), parts along dimension 0, may hold values from -6 to 6
- ffn_gain: float32 [2048], replicated, may hold values from 0.1 to 1.9
- expert_ids: int32 [32768, 2], P(('grp', 'ep', 'tp')), parts along dimension 0, may hold values from 0 to 31, all different within a row; in each aligned block of 128 rows (0 to 127, 128 to 255, ...) at most 12 rows name the same one
- expert_scores: float32 [32768, 2], P(('grp', 'ep', 'tp')), parts along dimension 0, may hold values from 0.05 to 1
- gate_weight: bfloat16 [32, 2048, 1024], P('ep', None, 'tp'), may hold values from -0.125 to 0.125
- up_weight: bfloat16 [32, 2048, 1024], P('ep', None, 'tp'), may hold values from -0.125 to 0.125
- down_weight: bfloat16 [32, 1024, 2048], P('ep', 'tp'), may hold values from -0.1875 to 0.1875
Outputs:
- mixed: bfloat16 [8192, 2048], P(('grp', 'ep', 'tp')), parts along dimension 0
- experts_mixed: bfloat16 [32768, 2048], P(('grp', 'ep', 'tp')), parts along dimension 0
There are 2 independent parts, one for each index of `grp`. A program takes and returns all parts, laid end to end along the dimension named above; an argument that names none is the same for every part. Nothing has to cross between parts.
Inputs may be any that keep to these rules, and one draw needn't show every extreme that they name: `expert_ids`: each token names 2 different experts. Among the 128 tokens of one device, no expert is named by more than 12 tokens, and in some device's tokens some expert is named by exactly 12.
All inputs are finite; a program needn't handle non-finite values.
Results may differ from a plain program's by a relative error of at most 0.012.
Values may be sent and summed in bfloat16 or wider, within the bound.
A program may use at most 128 MiB of HBM per device.

v0:
```python
import jax
import jax.numpy as jnp
from jax import lax
from jax.sharding import Mesh
from jax.sharding import PartitionSpec as P

EP = ("ep_0", "ep_1")
GRP_EP = ("grp", "ep_0", "ep_1")
GRP_EP_TP = ("grp", "ep_0", "ep_1", "tp")


def in_blocks(x, dim, devices):
    lengths = x.shape
    tiles = x.reshape(*lengths[:dim], devices, lengths[dim] // devices, *lengths[dim + 1 :])
    return jnp.moveaxis(tiles, dim, 0)


def joined_along(tiles, dim):
    lengths = list(tiles.shape[1:])
    lengths[dim] *= tiles.shape[0]
    return jnp.moveaxis(tiles, 0, dim).reshape(lengths)


def exchange_in_order(tiles, axes, sequence):
    lengths = [lax.axis_size(a) for a in axes]
    tiles = tiles.reshape(*lengths, *tiles.shape[1:])
    for k in sequence:
        tiles = lax.all_to_all(tiles, axes[k], split_axis=k, concat_axis=k, tiled=True)
    return tiles.reshape(-1, *tiles.shape[len(axes) :])


def two_step_exchange(x, groups, sequence, split_dim, concat_dim):
    devices = lax.axis_size(groups[0]) * lax.axis_size(groups[1])
    tiles = in_blocks(x, split_dim, devices)
    return joined_along(exchange_in_order(tiles, groups, sequence), concat_dim)


def gather_turned(arrays, axis, dims):
    turned = [jnp.moveaxis(a, dim, 0) for a, dim in zip(arrays, dims)]
    widths = [t[0].size for t in turned]
    both = jnp.concatenate([t.reshape(-1, w) for t, w in zip(turned, widths)], axis=1)
    whole = lax.all_gather(both, axis, axis=0, tiled=True)
    tiles = jnp.split(whole, [sum(widths[:k]) for k in range(1, len(widths))], axis=1)
    return tuple(
        (
            jnp.moveaxis(b.reshape(-1, *t.shape[1:]), 0, dim)
            for b, t, dim in zip(tiles, turned, dims)
        )
    )


def sent_together(arrays, axis, dim, along):
    both = jnp.concatenate(arrays, axis=along)
    whole, at, gathered = (lax.all_gather(both, axis, axis=dim, tiled=True), 0, [])
    for a in arrays:
        gathered.append(lax.slice_in_dim(whole, at, at + a.shape[along], axis=along))
        at += a.shape[along]
    return tuple(gathered)


def sum_at_owner(x, axis, dim):
    devices = lax.axis_size(axis)
    tiles = lax.all_to_all(in_blocks(x, dim, devices), axis, 0, 0, tiled=True)
    return jnp.sum(tiles.astype(jnp.float32), axis=0)


def norm_rows(values, gain):
    values = values.astype(jnp.float32)
    scale = lax.rsqrt(jnp.mean(values * values, axis=-1, keepdims=True) + 1e-06)
    return values * scale * gain


def break_terms(query_heads, query_place, key_block, bias_block, first):
    span = key_block.shape[0]
    heads = query_heads.shape[1]
    key_heads = key_block.reshape(span, heads, -1)
    scores = jnp.einsum("qhd,khd->hqk", query_heads, key_heads, preferred_element_type=jnp.float32)
    scores = scores * query_heads.shape[2] ** (-0.5) + bias_block.astype(jnp.float32).T[:, None, :]
    key_place = first + jnp.arange(span)
    past = (key_place[None, :] < query_place[:, None])[None]
    rest = jnp.where(past, jax.nn.log_sigmoid(-scores), 0.0)
    later = lax.cumsum(rest, axis=2, reverse=True)
    return (scores, past, rest, later)


def block_part(scores, past, rest, later, value_block, heads):
    within = later - rest
    local = jnp.where(past, jnp.exp(jax.nn.log_sigmoid(scores) + within), 0.0).astype(jnp.bfloat16)
    span = value_block.shape[0]
    value_heads = value_block.reshape(span, heads, -1)
    part = jnp.einsum("hqk,khd->qhd", local, value_heads, preferred_element_type=jnp.float32)
    return part.reshape(part.shape[0], -1)


def keep(state):
    return state


def dispatch_plan(normed, expert_ids, experts, capacity):
    rows, top = expert_ids.shape
    flat_ids = expert_ids.reshape(rows * top)
    onehot = (flat_ids[:, None] == jnp.arange(experts)[None, :]).astype(jnp.int32)
    earlier = jnp.cumsum(onehot, axis=0) - onehot
    place = jnp.sum(earlier * onehot, axis=1)
    target = flat_ids * capacity + place
    source = (
        jnp.zeros((experts * capacity,), jnp.int32)
        .at[target]
        .set(jnp.arange(rows * top, dtype=jnp.int32) // top + 1)
    )
    padded = jnp.concatenate([jnp.zeros((1, normed.shape[1]), normed.dtype), normed], axis=0)
    return (padded[source].reshape(experts, capacity, normed.shape[1]), target)


def expert_hidden(piece, gate_weight, up_weight):
    flat = piece.reshape(-1, piece.shape[-1])
    gate = jnp.dot(flat, gate_weight[0], preferred_element_type=jnp.float32)
    upward = jnp.dot(flat, up_weight[0], preferred_element_type=jnp.float32)
    hidden = (jax.nn.silu(gate) * upward).astype(jnp.bfloat16)
    return hidden.reshape(piece.shape[0], piece.shape[1], -1)


def send_back(summed):
    return two_step_exchange(summed.astype(jnp.bfloat16), ("ep_0", "ep_1"), (1, 0), 0, 0)


def serve_full(piece, whole_weights, groups):
    gate_full, up_full, down_full = whole_weights
    hidden = expert_hidden(piece, gate_full, up_full)
    flat = hidden.reshape(-1, hidden.shape[2])
    share = flat.shape[1] // groups
    summed = jnp.zeros((flat.shape[0], down_full.shape[2]), jnp.float32)
    for quarter in range(groups):
        term = jnp.dot(
            flat[:, quarter * share : (quarter + 1) * share],
            down_full[0, quarter * share : (quarter + 1) * share],
            preferred_element_type=jnp.float32,
        )
        summed = summed + term.astype(jnp.bfloat16).astype(jnp.float32)
    return send_back(summed.reshape(piece.shape[0], piece.shape[1], -1))


def per_device(
    queries,
    keys,
    values,
    stop_bias,
    out_weight,
    mix_gain,
    moe_input,
    ffn_gain,
    expert_ids,
    expert_scores,
    gate_weight,
    up_weight,
    down_weight,
):
    groups = lax.axis_size("tp")
    whole_weights = gather_turned((gate_weight, up_weight, down_weight), "tp", (2, 2, 1))
    span = queries.shape[0]
    heads = stop_bias.shape[1]
    width_heads = queries.shape[1]
    blocks = lax.axis_size(EP)
    own_first = lax.axis_index(EP) * span
    query_heads = queries.reshape(span, heads, -1)
    query_place = own_first + jnp.arange(span)

    def piece_rows(piece, index):
        return tuple((lax.dynamic_slice_in_dim(member, index * span, span, 0) for member in piece))

    start_state = (
        jnp.zeros((blocks, heads, span), jnp.float32),
        jnp.zeros((blocks, span, width_heads), jnp.float32),
    )
    piece = sent_together((keys, values, stop_bias), EP, 0, 1)

    def one_block(index, state):
        key_block, value_block, bias_block = piece_rows(piece, index)
        first = index * span

        def compute(inner_state):
            totals, parts = inner_state
            scores, past, rest, later = break_terms(
                query_heads, query_place, key_block, bias_block, first
            )
            part = block_part(scores, past, rest, later, value_block, heads)
            number = first // span
            totals = lax.dynamic_update_index_in_dim(totals, later[:, :, 0], number, 0)
            parts = lax.dynamic_update_index_in_dim(parts, part, number, 0)
            return (totals, parts)

        return lax.cond(first <= own_first, compute, keep, state)

    totals, parts = lax.fori_loop(0, piece[0].shape[0] // span, one_block, start_state)
    carried = lax.cumsum(totals, axis=0, reverse=True) - totals
    factor = jnp.exp(carried).transpose(0, 2, 1)[:, :, :, None]
    attended = jnp.sum(factor * parts.reshape(blocks, span, heads, -1), axis=0).reshape(
        span, width_heads
    )
    attended = attended.astype(jnp.bfloat16)
    projected = sum_at_owner(
        jnp.dot(attended, out_weight, preferred_element_type=jnp.float32).astype(jnp.bfloat16),
        "tp",
        0,
    )
    mixed = norm_rows(projected, mix_gain).astype(jnp.bfloat16)
    normed = norm_rows(moe_input, ffn_gain).astype(jnp.bfloat16)
    rows, top = expert_ids.shape
    experts = lax.axis_size(EP)
    capacity = 3 * rows * top // (2 * experts)
    weights = expert_scores / jnp.sum(expert_scores, axis=1, keepdims=True)
    outbound, target = dispatch_plan(normed, expert_ids, experts, capacity)
    returned = serve_full(
        lax.all_to_all(outbound, EP, split_axis=0, concat_axis=0, tiled=True), whole_weights, groups
    )
    picked = returned.reshape(experts * capacity, -1)[target].reshape(rows, top, -1)
    experts_mixed = jnp.sum(picked.astype(jnp.float32) * weights[:, :, None], axis=1).astype(
        jnp.bfloat16
    )
    return (mixed, experts_mixed)


def solution(mesh):
    finer = Mesh(
        mesh.devices.reshape(mesh.shape["grp"], 16, 2, mesh.shape["tp"]),
        ("grp", "ep_0", "ep_1", "tp"),
    )
    placed = (
        P(GRP_EP, "tp"),
        P(GRP_EP, "tp"),
        P(GRP_EP, "tp"),
        P(GRP_EP, "tp"),
        P("tp", None),
        P(),
        P(GRP_EP_TP, None),
        P(),
        P(GRP_EP_TP, None),
        P(GRP_EP_TP, None),
        P(EP, None, "tp"),
        P(EP, None, "tp"),
        P(EP, "tp", None),
    )
    return jax.shard_map(
        per_device,
        mesh=finer,
        in_specs=placed,
        out_specs=(P(GRP_EP_TP, None), P(GRP_EP_TP, None)),
        check_vma=False,
    )
```

profile of v0, /device:TPU:33, one launch (start us, length us, event | category | flops | bytes accessed | tf_op | source)
XLA Modules:
  0.0 493.6 jit_solution(11107196582437392876)
XLA Ops:
  14.8 3.0 pad_maximum_fusion
  22.0 3.1 gather_fusion
  25.2 3.7 reshape.165
  28.8 25.5 %all-to-all-start.1 = ((bf16[32,12,2048]{2,1,0:T(8,128)(2,1)}), bf16[32,12,2048]{2,1,0:T(8,128)(2,1)}, u32[]{:S(2)}, u32[]{:S(2)}) async-start(bf16[32,12,2048]{2,1,0:T(8,128)(2,1)} %reshape.165), calls=%async_computation.1 | async-start | bytes 4194304 | tf_op jit(solution)/shard_map/all_to_all | solution.py:214
  54.5 115.4 %all-to-all-done.1 = bf16[32,12,2048]{2,1,0:T(8,128)(2,1)} async-done(((bf16[32,12,2048]{2,1,0:T(8,128)(2,1)}), bf16[32,12,2048]{2,1,0:T(8,128)(2,1)}, u32[]{:S(2)}, u32[]{:S(2)}) %all-to-all-start.1) | async-done | bytes 1572896 | tf_op jit(solution)/shard_map/all_to_all | solution.py:214
  169.9 3.6 reshape.166
  173.5 24.6 %all-gather.3.cloned.1.call-done = bf16[4096,1032]{0,1:T(8,128)(2,1)} async-done(((bf16[128,1032]{0,1:T(8,128)(2,1)}), bf16[4096,1032]{0,1:T(8,128)(2,1)}) %all-gather.3.cloned.1.call-update) | async-done | bytes 8454160 | tf_op jit(solution)/shard_map/all_gather | solution.py:54
  198.9 6.0 %fusion.38 = (bf16[4096,512]{0,1:T(8,128)(2,1)}, bf16[4096,512]{0,1:T(8,128)(2,1)}) fusion(bf16[4096,1032]{0,1:T(8,128)(2,1)} %all-gather.3.cloned.1.call-done), kind=kLoop, calls=%fused_computation.91 | loop fusion | bytes 16777216 | tf_op jit(solution)/shard_map/slice | solution.py:56
  205.0 4.2 broadcast_in_dim.57
  209.1 10.8 %while.17 = (s32[]{:T(128)}, f32[32,8,128]{2,1,0:T(8,128)S(1)}, f32[32,128,512]{1,2,0:T(8,128)}, s32[]{:T(128)}, bf16[4096,512]{0,1:T(8,128)(2,1)}, /*index=5*/b...) while((s32[]{:T(128)}, f32[32,8,128]{2,1,0:T(8,128)S(1)}, ...), condition=%wide.region_4.5_spmd.clone.clone, body=%wide.region_0.4_spmd.clone.clone.sunk | while | flops 54150424 | bytes 4920800 | solution.py:194
  209.1 4.6 conditional.4
  213.7 4.6 conditional.4
  221.9 4.1 fusion.18
  227.3 93.0 %all-gather.5.cloned.1.call-done = bf16[1024,6144]{1,0:T(8,128)(2,1)} async-done(((bf16[256,6144]{1,0:T(8,128)(2,1)}), bf16[1024,6144]{1,0:T(8,128)(2,1)}) %all-gather.5.cloned.1.call-update) | async-done | bytes 12582928 | tf_op jit(solution)/shard_map/all_gather | solution.py:42
  322.8 4.0 fusion.20
  326.8 4.1 multiply_convert_fusion
  338.2 5.5 %all_to_all.20 = bf16[16,2,1,12,2048]{4,0,3,2,1:T(8,128)(2,1)S(1)} all-to-all(bf16[16,2,1,12,2048]{4,0,3,2,1:T(8,128)(2,1)S(1)} %copy.49), channel_id=1, replica_groups=mesh['grp'=2,'ep_0'=16,'ep_1'=2,'tp'=4] {'ep_1'}, dimensions={1} | all-to-all | bytes 3145728 | tf_op jit(solution)/shard_map/all_to_all | solution.py:28
  343.7 3.7 all-to-all-start
  347.4 2.8 copy.50
  350.2 6.1 %all-to-all-done = bf16[4,32,2048]{2,1,0:T(8,128)(2,1)S(1)} async-done(((bf16[4,32,2048]{2,1,0:T(8,128)(2,1)}), bf16[4,32,2048]{2,1,0:T(8,128)(2,1)S(1)}, u32[]{:S(2)}, u32[]{:S(2)}) %all-to-all-start) | async-done | bytes 524320 | tf_op jit(solution)/shard_map/all_to_all | solution.py:63
  356.3 45.7 %all-to-all-start.3 = ((bf16[16,2,1,12,2048]{4,1,3,2,0:T(2,128)(2,1)}), bf16[16,2,1,12,2048]{4,1,3,2,0:T(2,128)(2,1)}, u32[]{:S(2)}, u32[]{:S(2)}) async-start(bf16[16,2,1,12,2048]{4,1,3,2,0:T(2,128)(2,1)} %copy.50), calls=%async_computation.3 | async-start | bytes 3145728 | tf_op jit(solution)/shard_map/all_to_all | solution.py:28
  403.1 68.1 %all-to-all-done.3 = bf16[16,2,1,12,2048]{4,1,3,2,0:T(2,128)(2,1)} async-done(((bf16[16,2,1,12,2048]{4,1,3,2,0:T(2,128)(2,1)}), bf16[16,2,1,12,2048]{4,1,3,2,0:T(2,128)(2,1)}, u32[]{:S(2)}, u32[]{:S(2)}) %all-to-all-start.3) | async-done | bytes 1572896 | tf_op jit(solution)/shard_map/all_to_all | solution.py:28
  474.7 4.1 gather_fusion.1
  481.2 5.6 %multiply_reduce_fusion = bf16[128,2048]{1,0:T(8,128)(2,1)} fusion(f32[128,2,2048]{2,1,0:T(2,128)} %reshape.171, f32[128,2]{1,0:T(8,128)S(1)} %copy.52), kind=kLoop, calls=%fused_computation.44 | loop fusion | flops 786432 | bytes 2622464 | tf_op jit(solution)/shard_map/reduce_sum | solution.py:217
  (151 shorter events, 42.4 us)
Async XLA Ops:
  7.2 218.8 %copy-start = (bf16[512,2048]{1,0:T(8,128)(2,1)S(1)}, bf16[512,2048]{1,0:T(8,128)(2,1)}, u32[]{:S(2)}) copy-start(bf16[512,2048]{1,0:T(8,128)(2,1)} %param.21) | copy-start | bytes 6291460
  7.2 190.9 %all-gather.3.cloned.1.call-start = ((), (), s32[]{:S(2)}) async-start(), calls=%async_computation.4 | async-start | bytes 8718336 | tf_op jit(solution)/shard_map/all_gather | solution.py:54
  10.9 309.3 %all-gather.5.cloned.1.call-start = ((), (), s32[]{:S(2)}) async-start(), calls=%async_computation.5 | async-start | bytes 15728640 | tf_op jit(solution)/shard_map/all_gather | solution.py:42
  17.8 0.7 copy-start.7
  17.8 2.2 copy-start.2
  17.8 2.4 copy-start.5
  25.2 29.2 %copy-start.4 = (bf16[128,512]{1,0:T(8,128)(2,1)S(1)}, bf16[128,512]{1,0:T(8,128)(2,1)}, u32[]{:S(2)}) copy-start(bf16[128,512]{1,0:T(8,128)(2,1)} %param.17) | copy-start | bytes 393220
  28.8 141.1 %all-to-all-start.1 = ((bf16[32,12,2048]{2,1,0:T(8,128)(2,1)}), bf16[32,12,2048]{2,1,0:T(8,128)(2,1)}, u32[]{:S(2)}, u32[]{:S(2)}) async-start(bf16[32,12,2048]{2,1,0:T(8,128)(2,1)} %reshape.165), calls=%async_computation.1 | async-start | bytes 4194304 | tf_op jit(solution)/shard_map/all_to_all | solution.py:214
  227.3 95.5 %copy-start.3 = (bf16[384,2048]{1,0:T(8,128)(2,1)S(1)}, bf16[384,2048]{1,0:T(8,128)(2,1)}, u32[]{:S(2)}) copy-start(bf16[384,2048]{1,0:T(8,128)(2,1)} %reshape.166) | copy-start | bytes 4718596
  343.7 12.6 %all-to-all-start = ((bf16[4,32,2048]{2,1,0:T(8,128)(2,1)}), bf16[4,32,2048]{2,1,0:T(8,128)(2,1)S(1)}, u32[]{:S(2)}, u32[]{:S(2)}) async-start(bf16[4,32,2048]{2,1,0:T(8,128)(2,1)} %bitcast.10), calls=%async_computation | async-start | bytes 1048576 | tf_op jit(solution)/shard_map/all_to_all | solution.py:63
  347.4 54.6 %copy-start.8 = (f32[128,2]{0,1:T(2,128)S(1)}, f32[128,2]{0,1:T(2,128)}, u32[]{:S(2)}) copy-start(f32[128,2]{0,1:T(2,128)} %param.26) | copy-start | bytes 3076
  347.4 55.0 %copy-start.6 = (f32[2048]{0:T(1024)S(1)}, f32[2048]{0:T(1024)}, u32[]{:S(2)}) copy-start(f32[2048]{0:T(1024)} %param.22) | copy-start | bytes 24580
  356.3 114.9 %all-to-all-start.3 = ((bf16[16,2,1,12,2048]{4,1,3,2,0:T(2,128)(2,1)}), bf16[16,2,1,12,2048]{4,1,3,2,0:T(2,128)(2,1)}, u32[]{:S(2)}, u32[]{:S(2)}) async-start(bf16[16,2,1,12,2048]{4,1,3,2,0:T(2,128)(2,1)} %copy.50), calls=%async_computation.3 | async-start | bytes 3145728 | tf_op jit(solution)/shard_map/all_to_all | solution.py:28
  474.7 12.1 %copy-start.1 = (bf16[512,2048]{1,0:T(8,128)(2,1)S(1)}, bf16[512,2048]{1,0:T(8,128)(2,1)}, u32[]{:S(2)}) copy-start(bf16[512,2048]{1,0:T(8,128)(2,1)} %param.21) | copy-start | bytes 6291460
Sparse Core Ops, SparseCore 0:
  11.0 187.0 all-gather.2
  199.9 120.2 all-gather.4
where the time goes:
time: 499 us; the launch traced here: 494 us
  waiting for transfers between devices  307 us (62%)
  starting transfers between devices  75 us (15%)
  local copies, waits for them, and re-layouts  53 us (11%)
  other arithmetic  20.9 us (4%)
  matrix products  16 us (3%)
  between operations  14.4 us (3%)
  blocking collectives  5.48 us (1%)
    all_to_all x1, waiting for transfers between devices, per_device(): lax.all_to_all(outbound, EP, split_axis=0, concat_axis=0, tiled=True)  115 us
    all_gather x1, waiting for transfers between devices, gather_turned(): whole = lax.all_gather(both, axis, axis=0, tiled=True)  93 us
    all_to_all x1, waiting for transfers between devices, exchange_in_order(): lax.all_to_all(tiles, axes[k], split_axis=k, concat_axis=k, tiled=True)  68.1 us
    all_to_all x1, starting transfers between devices, exchange_in_order(): lax.all_to_all(tiles, axes[k], split_axis=k, concat_axis=k, tiled=True)  45.7 us
    all_to_all x1, starting transfers between devices, per_device(): lax.all_to_all(outbound, EP, split_axis=0, concat_axis=0, tiled=True)  25.5 us
    all_gather x1, waiting for transfers between devices, sent_together(): lax.all_gather(both, axis, axis=dim, tiled=True)  24.6 us
  transfers between devices with their start and end apart: 5, of which 5 were waited for; matrix products, arithmetic and copies ran while one was open for 11% of the time, Pallas kernels for 0%

commit v1 on v0

v1 whole, which is shorter than its diff:
```python
import functools

import jax
import jax.numpy as jnp
from jax import lax
from jax.experimental import pallas as pl
from jax.experimental.pallas import tpu as pltpu
from jax.sharding import PartitionSpec as P

MESH = pl.DeviceIdType.MESH
BF16 = jnp.bfloat16
F32 = jnp.float32
GRP_EP = ("grp", "ep")
GRP_EP_TP = ("grp", "ep", "tp")
ROWS = 8


def dot(a, b):
    return jnp.dot(a, b, preferred_element_type=F32)


def iota(shape, dim):
    return lax.broadcasted_iota(jnp.int32, shape, dim)


def half_turn(x):
    return jnp.concatenate([x[4:], x[:4]], axis=0)


def norm_rows(values, gain):
    scale = lax.rsqrt(jnp.mean(values * values, axis=-1, keepdims=True) + 1e-06)
    return values * scale * gain


def kernel(
    n, t,
    q_ref, k_ref, v_ref, bias_ref, ow_ref, mix_gain_ref, x_ref, ffn_gain_ref, ids_ref, score_ref, gw_ref, uw_ref, dw_ref,
    mixed_ref, moe_ref,
    gate, up, down, ow, kv, qm, acc, carry, out_buf, in_buf, back, ret, xb, total, marks, proj, proj_in,
    loc_sem, w_send, w_recv, f_send, f_recv, kv_send, kv_recv, d_send, d_recv, r_send, r_recv, p_send, p_recv,
):
    me, col = lax.axis_index("ep"), lax.axis_index("tp")
    span, width = q_ref.shape
    tokens, model = x_ref.shape
    heads = bias_ref.shape[0]
    pairs = heads // 2
    wide = model + model // 2
    right, left = lax.rem(col + 1, t), lax.rem(col + t - 1, t)
    far = lax.rem(col + 2, t)
    core = lax.rem(me, 2)
    partner = me + 1 - 2 * core
    chips = n // 2
    plus_steps, minus_steps = chips // 2, (chips - 1) // 2

    barrier = pltpu.get_barrier_semaphore()

    def greet(d, _):
        pl.semaphore_signal(barrier, inc=1, device_id={"ep": lax.rem(me + d, n)}, device_id_type=MESH)
        return 0

    lax.fori_loop(1, n, greet, 0)
    for d in range(1, t):
        pl.semaphore_signal(barrier, inc=1, device_id={"tp": lax.rem(col + d, t)}, device_id_type=MESH)

    local = [
        pltpu.make_async_copy(k_ref, kv.at[me, pl.ds(0, span)], loc_sem.at[0]),
        pltpu.make_async_copy(v_ref, kv.at[me, pl.ds(span, span)], loc_sem.at[1]),
        pltpu.make_async_copy(gw_ref.at[0], gate.at[col], loc_sem.at[2]),
        pltpu.make_async_copy(uw_ref.at[0], up.at[col], loc_sem.at[3]),
        pltpu.make_async_copy(dw_ref.at[0], down.at[col], loc_sem.at[4]),
        pltpu.make_async_copy(ow_ref, ow, loc_sem.at[5]),
    ]
    for c in local:
        c.start()
    kv[me, pl.ds(2 * span, ROWS), :] = jnp.zeros((ROWS, width), BF16)
    kv[me, pl.ds(2 * span, ROWS), 0:span] = bias_ref[...]

    normed = norm_rows(x_ref[...].astype(F32), ffn_gain_ref[...]).astype(BF16)
    first, second = ids_ref[0:1, :], ids_ref[1:2, :]
    expert = iota((n, tokens), 0)
    named0, named1 = expert == first, expert == second
    named = jnp.where(named0 | named1, 1.0, 0.0)
    before = jnp.where(iota((tokens, tokens), 0) < iota((tokens, tokens), 1), 1.0, 0.0).astype(BF16)
    place = dot(named.astype(BF16), before)
    place = jnp.where(named > 0.5, place, 127.0)
    scores = score_ref[...]
    weights = scores / jnp.sum(scores, axis=0, keepdims=True)
    weight = jnp.where(named0, weights[0:1, :], 0.0) + jnp.where(named1, weights[1:2, :], 0.0)
    high = weight.astype(BF16)
    low = (weight - high.astype(F32)).astype(BF16)
    slots = n * ROWS
    spread = jnp.where(iota((slots, n), 0) // ROWS == iota((slots, n), 1), 1.0, 0.0).astype(BF16)
    place = dot(spread, place.astype(BF16))
    high, low = dot(spread, high), dot(spread, low)
    row = lax.rem(iota((slots, tokens), 0), ROWS)
    rowf = row.astype(F32)
    main = jnp.where(place == rowf, 1.0, 0.0)
    upper = jnp.where((row < 4) & (place == rowf + 8.0), 1.0, 0.0)
    lower = jnp.where((row >= 4) & (place == rowf + 4.0), 1.0, 0.0)
    for i, m in enumerate((main, upper, lower)):
        marks[i, 0] = (m * high).T.astype(BF16)
        marks[i, 1] = (m * low).T.astype(BF16)
    half = model // 2
    out_buf[:, 0:model] = dot(main.astype(BF16), normed).astype(BF16)
    out_buf[:, model:wide] = (
        dot(upper.astype(BF16), normed[:, 0:half]) + dot(lower.astype(BF16), normed[:, half:model])
    ).astype(BF16)

    pl.semaphore_wait(barrier, n - 1 + t - 1)

    def rows_of(ref, slot, part):
        size = ref.shape[1] // 2
        return ref.at[slot, pl.ds(part * size, size)]

    weight_set = ((gw_ref, gate), (uw_ref, up), (dw_ref, down))

    def direct(w, way, part):
        src, dst = weight_set[w]
        return pltpu.make_async_remote_copy(
            src_ref=rows_of(src, 0, part), dst_ref=rows_of(dst, col, part),
            send_sem=w_send.at[way, w, part], recv_sem=w_recv.at[way, w, part],
            device_id={"tp": right if way == 0 else left}, device_id_type=MESH,
        )

    def arrived(w, way, part):
        src, dst = weight_set[w]
        return pltpu.make_async_remote_copy(
            src_ref=rows_of(src, 0, part), dst_ref=rows_of(dst, left if way == 0 else right, part),
            send_sem=w_send.at[way, w, part], recv_sem=w_recv.at[way, w, part],
            device_id={"tp": right if way == 0 else left}, device_id_type=MESH,
        )

    def forward(w, way):
        dst = weight_set[w][1]
        held = rows_of(dst, left if way == 0 else right, way)
        return pltpu.make_async_remote_copy(
            src_ref=held, dst_ref=held, send_sem=f_send.at[way, w], recv_sem=f_recv.at[way, w],
            device_id={"tp": right if way == 0 else left}, device_id_type=MESH,
        )

    def forwarded(w, way):
        dst = weight_set[w][1]
        held = rows_of(dst, far, way)
        return pltpu.make_async_remote_copy(
            src_ref=held, dst_ref=held, send_sem=f_send.at[way, w], recv_sem=f_recv.at[way, w],
            device_id={"tp": right if way == 0 else left}, device_id_type=MESH,
        )

    for part in range(2):
        for w in range(3):
            for way in range(2):
                direct(w, way, part if way == 0 else 1 - part).start()

    def kv_copy(slot, way):
        peer = (lax.rem(me + 2, n), lax.rem(me + n - 2, n), partner)[way]
        return pltpu.make_async_remote_copy(
            src_ref=kv.at[slot], dst_ref=kv.at[slot], send_sem=kv_send.at[way, slot], recv_sem=kv_recv.at[slot],
            device_id={"ep": peer}, device_id_type=MESH,
        )

    local[0].wait()
    local[1].wait()
    kv_copy(me, 0).start()
    if minus_steps > 0:
        kv_copy(me, 1).start()
    kv_copy(me, 2).start()

    def strip(ref, index):
        return ref.at[pl.ds(pl.multiple_of(index * ROWS, ROWS), ROWS)]

    def dispatch(peer):
        return pltpu.make_async_remote_copy(
            src_ref=strip(out_buf, peer), dst_ref=strip(in_buf, me), send_sem=d_send.at[peer], recv_sem=d_recv.at[me],
            device_id={"ep": peer}, device_id_type=MESH,
        )

    def dispatched(peer):
        return pltpu.make_async_remote_copy(
            src_ref=strip(out_buf, peer), dst_ref=strip(in_buf, peer), send_sem=d_send.at[peer], recv_sem=d_recv.at[peer],
            device_id={"ep": peer}, device_id_type=MESH,
        )

    def give_back(peer):
        return pltpu.make_async_remote_copy(
            src_ref=strip(back, peer), dst_ref=strip(ret, me), send_sem=r_send.at[peer], recv_sem=r_recv.at[me],
            device_id={"ep": peer}, device_id_type=MESH,
        )

    def given_back(peer):
        return pltpu.make_async_remote_copy(
            src_ref=strip(back, peer), dst_ref=strip(ret, peer), send_sem=r_send.at[peer], recv_sem=r_recv.at[peer],
            device_id={"ep": peer}, device_id_type=MESH,
        )

    def at_distance(i):
        step = (i + 1) // 2
        return lax.rem(me + jnp.where(lax.rem(i, 2) == 1, step, n - step), n)

    def each_peer(act):
        def body(i, _):
            act(at_distance(i))
            return 0

        lax.fori_loop(1, n, body, 0)

    each_peer(lambda peer: dispatch(peer).start())
    own_in = pltpu.make_async_copy(strip(out_buf, me), strip(in_buf, me), loc_sem.at[6])
    own_in.start()

    lane = iota((span, 2 * (width // heads)), 1)
    headed = width // heads
    for p in range(pairs):
        both = q_ref[:, 2 * headed * p : 2 * headed * (p + 1)].astype(F32) * headed ** (-0.5)
        qm[p, 0:span] = jnp.where(lane < headed, both, 0.0).astype(BF16)
        qm[p, span : 2 * span] = jnp.where(lane >= headed, both, 0.0).astype(BF16)
    acc[...] = jnp.zeros_like(acc)
    carry[...] = jnp.zeros_like(carry)

    for w in range(3):
        arrived(w, 0, 0).wait_recv()
        forward(w, 0).start()
        arrived(w, 1, 1).wait_recv()
        forward(w, 1).start()

    each_peer(lambda peer: dispatched(peer).wait_recv())
    own_in.wait()

    def kv_step(k):
        if k <= plus_steps:
            slot = lax.rem(me + n - 2 * k, n)
            kv_copy(slot, 0).wait_recv()
            if k < plus_steps:
                kv_copy(slot, 0).start()
            kv_copy(slot, 2).start()
        if k <= minus_steps:
            slot = lax.rem(me + 2 * k, n)
            kv_copy(slot, 1).wait_recv()
            if k < minus_steps:
                kv_copy(slot, 1).start()
            kv_copy(slot, 2).start()

    kv_step(1)

    xb[0:slots] = in_buf[:, 0:model]
    row8 = iota((ROWS, half), 0)

    def join(i, _):
        base = pl.multiple_of(i * 4 * ROWS, 4 * ROWS)
        four = in_buf[pl.ds(base, 4 * ROWS), model:wide].astype(F32)
        lefts, rights = [], []
        for j in range(2):
            even, odd = four[2 * ROWS * j : 2 * ROWS * j + ROWS], four[2 * ROWS * j + ROWS : 2 * ROWS * (j + 1)]
            lefts.append(jnp.where(row8 < 4, even, half_turn(odd)))
            rights.append(jnp.where(row8 < 4, half_turn(even), odd))
        to = pl.ds(pl.multiple_of(slots + i * 2 * ROWS, 2 * ROWS), 2 * ROWS)
        xb[to, 0:half] = jnp.concatenate(lefts, axis=0).astype(BF16)
        xb[to, half:model] = jnp.concatenate(rights, axis=0).astype(BF16)
        return 0

    lax.fori_loop(0, n // 4, join, 0)

    chunk = 512

    def serve(slot, number):
        rows = xb[...]
        g = dot(rows, gate[slot])
        u = dot(rows, up[slot])
        hidden = (g / (1.0 + jnp.exp(-g)) * u).astype(BF16)
        for c in range(model // chunk):
            at = slice(c * chunk, (c + 1) * chunk)
            term = dot(hidden, down[slot, :, at]).astype(BF16).astype(F32)
            if number == 0:
                total[:, at] = term
            else:
                total[:, at] += term

    for c in local[2:5]:
        c.wait()
    serve(col, 0)
    kv_step(2)
    for w in range(3):
        arrived(w, 0, 1).wait_recv()
    serve(left, 1)
    kv_step(3)
    for w in range(3):
        arrived(w, 1, 0).wait_recv()
    serve(right, 2)
    for k in range(4, 7):
        kv_step(k)
    for w in range(3):
        forwarded(w, 0).wait_recv()
        forwarded(w, 1).wait_recv()
    serve(far, 3)
    back[:, 0:model] = total[0:slots].astype(BF16)

    def part(i, _):
        at = pl.ds(pl.multiple_of(slots + i * ROWS, ROWS), ROWS)
        lefts, rights = total[at, 0:half], total[at, half:model]
        even = jnp.where(row8 < 4, lefts, half_turn(rights))
        odd = jnp.where(row8 < 4, half_turn(lefts), rights)
        to = pl.ds(pl.multiple_of(i * 2 * ROWS, 2 * ROWS), 2 * ROWS)
        back[to, model:wide] = jnp.concatenate([even, odd], axis=0).astype(BF16)
        return 0

    lax.fori_loop(0, n // 2, part, 0)
    each_peer(lambda peer: give_back(peer).start())
    own_back = pltpu.make_async_copy(strip(back, me), strip(ret, me), loc_sem.at[7])
    own_back.start()
    for k in range(7, plus_steps + 1):
        kv_step(k)

    def from_partner(i, _):
        kv_copy(2 * i + 1 - core, 2).wait_recv()
        return 0

    lax.fori_loop(0, chips, from_partner, 0)

    later = jnp.where(iota((2 * span, 2 * span), 0) % span > iota((2 * span, 2 * span), 1), 1.0, 0.0)
    later = jnp.where(iota((2 * span, 2 * span), 1) >= span, 1.0, later).astype(BF16)
    past = iota((2 * span, span), 1) < lax.rem(iota((2 * span, span), 0), span)

    def attend(block, masked):
        for p in range(pairs):
            lanes = slice(2 * headed * p, 2 * headed * (p + 1))
            z = lax.dot_general(
                qm[p], kv[block, 0:span, lanes], (((1,), (1,)), ((), ())), preferred_element_type=F32
            )
            bias = kv[block, 2 * span : 2 * span + ROWS, 0:span].astype(F32)
            z = jnp.concatenate(
                [z[0:span] + bias[2 * p : 2 * p + 1], z[span : 2 * span] + bias[2 * p + 1 : 2 * p + 2]], axis=0
            )
            soft = jnp.log(1.0 + jnp.exp(-jnp.abs(z)))
            rest = jnp.minimum(-z, 0.0) - soft
            if masked:
                rest = jnp.where(past, rest, 0.0)
            top = rest.astype(BF16)
            bottom = (rest - top.astype(F32)).astype(BF16)
            sums = dot(jnp.concatenate([top, bottom], axis=1), later)
            power = jnp.exp(jnp.minimum(z, 0.0) - soft + (sums[:, 0:span] + carry[p]))
            if masked:
                power = jnp.where(past, power, 0.0)
            carry[p] += sums[:, span : 2 * span]
            acc[p] += dot(power.astype(BF16), kv[block, span : 2 * span, lanes])

    attend(me, True)

    def earlier(i, _):
        attend(me - 1 - i, False)
        return 0

    lax.fori_loop(0, me, earlier, 0)

    attended = jnp.concatenate(
        [jnp.where(lane < headed, acc[p, 0:span], acc[p, span : 2 * span]) for p in range(pairs)], axis=1
    ).astype(BF16)
    local[5].wait()
    share = span // t
    proj[...] = dot(attended, ow[...]).astype(BF16)

    def shares(ref, index):
        return ref.at[pl.ds(pl.multiple_of(index * share, share), share)]

    def project(peer, slot):
        return pltpu.make_async_remote_copy(
            src_ref=shares(proj, peer), dst_ref=shares(proj_in, slot), send_sem=p_send.at[peer], recv_sem=p_recv.at[slot],
            device_id={"tp": peer}, device_id_type=MESH,
        )

    own_share = pltpu.make_async_copy(shares(proj, col), shares(proj_in, col), loc_sem.at[8])
    own_share.start()
    for d in range(1, t):
        project(lax.rem(col + d, t), col).start()
    own_share.wait()
    for d in range(1, t):
        peer = lax.rem(col + d, t)
        project(peer, peer).wait_recv()
    projected = proj_in[0:share].astype(F32)
    for i in range(1, t):
        projected = projected + proj_in[i * share : (i + 1) * share].astype(F32)
    mixed_ref[...] = norm_rows(projected, mix_gain_ref[...]).astype(BF16)

    each_peer(lambda peer: given_back(peer).wait_recv())
    own_back.wait()
    for c in range(2):
        at = slice(c * half, (c + 1) * half)
        tail = ret[:, model:wide]
        mix = dot(marks[0, 0], ret[:, at]) + dot(marks[0, 1], ret[:, at])
        mix = mix + dot(marks[1 + c, 0], tail) + dot(marks[1 + c, 1], tail)
        moe_ref[:, at] = mix.astype(BF16)

    for w in range(3):
        for way in range(2):
            forward(w, way).wait_send()
            for s in range(2):
                direct(w, way, s).wait_send()

    def left_here(peer):
        dispatch(peer).wait_send()
        give_back(peer).wait_send()

    each_peer(left_here)
    for k in range(plus_steps):
        kv_copy(lax.rem(me + n - 2 * k, n), 0).wait_send()
    for k in range(minus_steps):
        kv_copy(lax.rem(me + 2 * k, n), 1).wait_send()

    def to_partner(i, _):
        kv_copy(2 * i + core, 2).wait_send()
        return 0

    lax.fori_loop(0, chips, to_partner, 0)
    for d in range(1, t):
        project(lax.rem(col + d, t), col).wait_send()


def per_device(
    queries, keys, values, stop_bias, out_weight, mix_gain, moe_input, ffn_gain, expert_ids, expert_scores,
    gate_weight, up_weight, down_weight,
):
    n, t = lax.axis_size("ep"), lax.axis_size("tp")
    span, width = queries.shape
    heads = stop_bias.shape[1]
    tokens, model = moe_input.shape
    hidden = gate_weight.shape[2]
    slots, wide, pairs = n * ROWS, model + model // 2, heads // 2
    vmem, anywhere = pl.BlockSpec(memory_space=pltpu.VMEM), pl.BlockSpec(memory_space=pl.ANY)
    dma = pltpu.SemaphoreType.DMA
    return pl.pallas_call(
        functools.partial(kernel, n, t),
        out_shape=(
            jax.ShapeDtypeStruct((span // t, model), BF16),
            jax.ShapeDtypeStruct((tokens, model), BF16),
        ),
        in_specs=[
            vmem, anywhere, anywhere, vmem, anywhere, vmem, vmem, vmem, vmem, vmem, anywhere, anywhere, anywhere,
        ],
        out_specs=(vmem, vmem),
        scratch_shapes=[
            pltpu.VMEM((t, model, hidden), BF16),
            pltpu.VMEM((t, model, hidden), BF16),
            pltpu.VMEM((t, hidden, model), BF16),
            pltpu.VMEM(out_weight.shape, BF16),
            pltpu.VMEM((n, 2 * span + ROWS, width), BF16),
            pltpu.VMEM((pairs, 2 * span, 2 * width // heads), BF16),
            pltpu.VMEM((pairs, 2 * span, 2 * width // heads), F32),
            pltpu.VMEM((pairs, 2 * span, span), F32),
            pltpu.VMEM((slots, wide), BF16),
            pltpu.VMEM((slots, wide), BF16),
            pltpu.VMEM((slots, wide), BF16),
            pltpu.VMEM((slots, wide), BF16),
            pltpu.VMEM((slots + slots // 2, model), BF16),
            pltpu.VMEM((slots + slots // 2, model), F32),
            pltpu.VMEM((3, 2, tokens, slots), BF16),
            pltpu.VMEM((span, model), BF16),
            pltpu.VMEM((span, model), BF16),
            dma((9,)),
            dma((2, 3, 2)),
            dma((2, 3, 2)),
            dma((2, 3)),
            dma((2, 3)),
            dma((3, n)),
            dma((n,)),
            dma((n,)),
            dma((n,)),
            dma((n,)),
            dma((n,)),
            dma((t,)),
            dma((t,)),
        ],
        compiler_params=pltpu.CompilerParams(
            collective_id=0, has_side_effects=True, vmem_limit_bytes=60 * 1024 * 1024
        ),
    )(
        queries, keys, values, stop_bias.T, out_weight, mix_gain[None, :], moe_input, ffn_gain[None, :],
        expert_ids.T, expert_scores.T, gate_weight, up_weight, down_weight,
    )


def solution(mesh):
    placed = (
        P(GRP_EP, "tp"), P(GRP_EP, "tp"), P(GRP_EP, "tp"), P(GRP_EP, "tp"), P("tp", None), P(), P(GRP_EP_TP, None), P(),
        P(GRP_EP_TP, None), P(GRP_EP_TP, None), P("ep", None, "tp"), P("ep", None, "tp"), P("ep", "tp", None),
    )
    return jax.shard_map(
        per_device,
        mesh=mesh,
        in_specs=placed,
        out_specs=(P(GRP_EP_TP, None), P(GRP_EP_TP, None)),
        check_vma=False,
    )
```

time: 499 us -> 268 us (0.54)
  the two profiles are of different devices: /device:TPU:33 before, /device:TPU:1953 now
where the time goes in v1:
time: 268 us
  Pallas kernels  263 us (98%)
  local copies, waits for them, and re-layouts  3.45 us (1%)
    pallas_call x1, Pallas kernels, per_device(): pl.pallas_call(functools.partial(kernel, n, t), out_shape=(jax.ShapeDtype...  263 us

profile of v1, /device:TPU:1953, one launch (start us, length us, event | category | flops | bytes accessed | tf_op | source)
XLA Modules:
  0.0 267.5 jit_solution(5985105395932398574)
XLA Ops:
  0.6 263.4 %shard_map.140 = (bf16[32,2048]{1,0:T(8,128)(2,1)}, bf16[128,2048]{1,0:T(8,128)(2,1)}) custom-call(bf16[128,512]{1,0:T(8,128)(2,1)} %q_ref.1, bf16[128,512]{1,0:T(8,128)(2,1)} %k_ref.1, bf16[128,512]{1,0:T(8,128)(2,1)} %v_ref.1, bf16[8,128]{1,0:T(8,128)(2,1)} %bitcast.7, bf16[512,2048]{1,0:T(8,128)(2,1)} %ow_ref.1, f32[1,2048]{1,0:T(1,128)} %bitcast.5, ...), custom_call_target="tpu_custom_call" | custom-call | tf_op jit(solution)/shard_map/pallas_call | solution.py:428
  264.1 1.6 copy.17
  265.6 1.9 copy.18

commit v2 on v1

v2 whole, which is shorter than its diff:
```python
import contextlib
import functools

import jax
import jax.numpy as jnp
from jax import lax
from jax.experimental import pallas as pl
from jax.experimental.pallas import tpu as pltpu
from jax.sharding import PartitionSpec as P

MESH = pl.DeviceIdType.MESH
BF16 = jnp.bfloat16
F32 = jnp.float32
GRP_EP = ("grp", "ep")
GRP_EP_TP = ("grp", "ep", "tp")
ROWS = 8


def scope(name):
    return contextlib.nullcontext()


def dot(a, b):
    return jnp.dot(a, b, preferred_element_type=F32)


def iota(shape, dim):
    return lax.broadcasted_iota(jnp.int32, shape, dim)


def half_turn(x):
    return jnp.concatenate([x[4:], x[:4]], axis=0)


def norm_rows(values, gain):
    scale = lax.rsqrt(jnp.mean(values * values, axis=-1, keepdims=True) + 1e-06)
    return values * scale * gain


def kernel(
    n, t,
    q_ref, k_ref, v_ref, bias_ref, ow_ref, mix_gain_ref, x_ref, ffn_gain_ref, ids_ref, score_ref, gw_ref, uw_ref, dw_ref,
    mixed_ref, moe_ref,
    gate, up, down, ow, q_out, q_in, kv_out, kv_in, a_out, a_in, qm, acc, carry,
    out_buf, in_buf, back, ret, xb, total, marks, proj, proj_in,
    loc_sem, w_send, w_recv, f_send, f_recv, q_send, q_recv, kv_send, kv_recv, c_send, a_send, a_recv,
    d_send, d_recv, r_send, r_recv, p_send, p_recv,
):
    me, col = lax.axis_index("ep"), lax.axis_index("tp")
    span, width = q_ref.shape
    tokens, model = x_ref.shape
    heads = bias_ref.shape[0]
    headed = width // heads
    pairs = heads // 2
    wide = model + model // 2
    right, left = lax.rem(col + 1, t), lax.rem(col + t - 1, t)
    far = lax.rem(col + 2, t)
    core = lax.rem(me, 2)
    partner = me + 1 - 2 * core
    crew = n // heads
    head, member = me // crew, lax.rem(me, crew)

    barrier = pltpu.get_barrier_semaphore()

    def greet(d, _):
        pl.semaphore_signal(barrier, inc=1, device_id={"ep": lax.rem(me + d, n)}, device_id_type=MESH)
        return 0

    lax.fori_loop(1, n, greet, 0)
    for d in range(1, t):
        pl.semaphore_signal(barrier, inc=1, device_id={"tp": lax.rem(col + d, t)}, device_id_type=MESH)

    local = [
        pltpu.make_async_copy(gw_ref.at[0], gate.at[col], loc_sem.at[2]),
        pltpu.make_async_copy(uw_ref.at[0], up.at[col], loc_sem.at[3]),
        pltpu.make_async_copy(dw_ref.at[0], down.at[col], loc_sem.at[4]),
        pltpu.make_async_copy(ow_ref, ow, loc_sem.at[5]),
    ]
    for c in local:
        c.start()

    side = span // 2
    lane = iota((span, 2 * headed), 1)
    lane_side = iota((side, 2 * headed), 1)
    swap = functools.partial(pltpu.roll, shift=headed, axis=1)
    with scope("pack"):
        for p in range(pairs):
            lanes = slice(2 * headed * p, 2 * headed * (p + 1))
            q = q_ref[:, lanes].astype(F32) * headed ** (-0.5)
            k, v = k_ref[:, lanes].astype(F32), v_ref[:, lanes].astype(F32)
            q_out[2 * p] = jnp.where(lane_side < headed, q[0:side], swap(q[side:span])).astype(BF16)
            q_out[2 * p + 1] = jnp.where(lane_side < headed, swap(q[0:side]), q[side:span]).astype(BF16)
            kv_out[2 * p, 0:span] = jnp.where(lane < headed, k, swap(v)).astype(BF16)
            kv_out[2 * p + 1, 0:span] = jnp.where(lane < headed, swap(k), v).astype(BF16)
        odds = bias_ref[...].astype(F32)
        for h in range(heads):
            kv_out[h, span : span + ROWS] = jnp.broadcast_to(odds[h : h + 1], (ROWS, span)).astype(BF16)

    with scope("plan"):
        normed = norm_rows(x_ref[...].astype(F32), ffn_gain_ref[...]).astype(BF16)
        first, second = ids_ref[0:1, :], ids_ref[1:2, :]
        expert = iota((n, tokens), 0)
        named0, named1 = expert == first, expert == second
        named = jnp.where(named0 | named1, 1.0, 0.0)
        before = jnp.where(iota((tokens, tokens), 0) < iota((tokens, tokens), 1), 1.0, 0.0).astype(BF16)
        place = dot(named.astype(BF16), before)
        place = jnp.where(named > 0.5, place, 127.0)
        scores = score_ref[...]
        weights = scores / jnp.sum(scores, axis=0, keepdims=True)
        weight = jnp.where(named0, weights[0:1, :], 0.0) + jnp.where(named1, weights[1:2, :], 0.0)
        high = weight.astype(BF16)
        low = (weight - high.astype(F32)).astype(BF16)
        slots = n * ROWS
        spread = jnp.where(iota((slots, n), 0) // ROWS == iota((slots, n), 1), 1.0, 0.0).astype(BF16)
        place = dot(spread, place.astype(BF16))
        high, low = dot(spread, high), dot(spread, low)
        row = lax.rem(iota((slots, tokens), 0), ROWS)
        rowf = row.astype(F32)
        main = jnp.where(place == rowf, 1.0, 0.0)
        upper = jnp.where((row < 4) & (place == rowf + 8.0), 1.0, 0.0)
        lower = jnp.where((row >= 4) & (place == rowf + 4.0), 1.0, 0.0)
        for i, m in enumerate((main, upper, lower)):
            marks[i, 0] = (m * high).T.astype(BF16)
            marks[i, 1] = (m * low).T.astype(BF16)
        half = model // 2
        out_buf[:, 0:model] = dot(main.astype(BF16), normed).astype(BF16)
        out_buf[:, model:wide] = (
            dot(upper.astype(BF16), normed[:, 0:half]) + dot(lower.astype(BF16), normed[:, half:model])
        ).astype(BF16)

    with scope("barrier"):
        pl.semaphore_wait(barrier, n - 1 + t - 1)

    def rows_of(ref, slot, part):
        size = ref.shape[1] // 2
        return ref.at[slot, pl.ds(part * size, size)]

    weight_set = ((gw_ref, gate), (uw_ref, up), (dw_ref, down))

    def side_copy(src, dst, sends, recvs, way):
        return pltpu.make_async_remote_copy(
            src_ref=src, dst_ref=dst, send_sem=sends, recv_sem=recvs,
            device_id={"tp": right if way == 0 else left}, device_id_type=MESH,
        )

    def direct(w, way, part, slot=col):
        src, dst = weight_set[w]
        return side_copy(
            rows_of(src, 0, part), rows_of(dst, slot, part), w_send.at[way, w, part], w_recv.at[way, w, part], way
        )

    def arrived(w, way, part):
        return direct(w, way, part, left if way == 0 else right)

    def forward(w, way, slot=None):
        held = rows_of(weight_set[w][1], (left if way == 0 else right) if slot is None else slot, way)
        return side_copy(held, held, f_send.at[way, w], f_recv.at[way, w], way)

    def forwarded(w, way):
        return forward(w, way, far)

    for part in range(2):
        for w in range(3):
            for way in range(2):
                direct(w, way, part if way == 0 else 1 - part).start()

    def along(src, dst, sends, recvs, peer):
        return pltpu.make_async_remote_copy(
            src_ref=src, dst_ref=dst, send_sem=sends, recv_sem=recvs, device_id={"ep": peer}, device_id_type=MESH
        )

    def send_q(h):
        return along(q_out.at[h], q_in.at[head], q_send.at[h], q_recv.at[head], crew * h + member)

    def got_q(j):
        return along(q_out.at[j], q_in.at[j], q_send.at[j], q_recv.at[j], crew * j + member)

    def send_kv(h, c):
        return along(kv_out.at[h], kv_in.at[me], kv_send.at[h, c], kv_recv.at[me], crew * h + 2 * c + core)

    def got_kv(source):
        return along(kv_out.at[0], kv_in.at[source], kv_send.at[0, 0], kv_recv.at[source], partner)

    def share_kv(source):
        return along(kv_in.at[source], kv_in.at[source], c_send.at[source], kv_recv.at[source], partner)

    chip, chips = member // 2, crew // 2
    order = sorted(range(1, heads), key=lambda d: (min(d, heads - d), d))
    own_q = pltpu.make_async_copy(q_out.at[head], q_in.at[head], loc_sem.at[0])
    own_kv = pltpu.make_async_copy(kv_out.at[head], kv_in.at[me], loc_sem.at[1])
    own_q.start()
    own_kv.start()
    for d in order:
        h = lax.rem(head + d, heads)
        for c in range(chips):
            send_kv(h, c).start()
        send_q(h).start()
    for c in range(1, chips):
        send_kv(head, lax.rem(chip + c, chips)).start()

    def strip(ref, index):
        return ref.at[pl.ds(pl.multiple_of(index * ROWS, ROWS), ROWS)]

    def dispatch(peer):
        return along(strip(out_buf, peer), strip(in_buf, me), d_send.at[peer], d_recv.at[me], peer)

    def dispatched(peer):
        return along(strip(out_buf, peer), strip(in_buf, peer), d_send.at[peer], d_recv.at[peer], peer)

    def give_back(peer):
        return along(strip(back, peer), strip(ret, me), r_send.at[peer], r_recv.at[me], peer)

    def given_back(peer):
        return along(strip(back, peer), strip(ret, peer), r_send.at[peer], r_recv.at[peer], peer)

    def each_peer(act):
        def body(i, _):
            step = (i + 1) // 2
            act(lax.rem(me + jnp.where(lax.rem(i, 2) == 1, step, n - step), n))
            return 0

        lax.fori_loop(1, n, body, 0)

    with scope("issue"):
        each_peer(lambda peer: dispatch(peer).start())
        own_in = pltpu.make_async_copy(strip(out_buf, me), strip(in_buf, me), loc_sem.at[6])
        own_in.start()

    acc[...] = jnp.zeros_like(acc)
    carry[...] = jnp.zeros_like(carry)

    with scope("kvwait"):
        own_kv.wait()
        share_kv(me).start()

        def pass_on(i, _):
            source = lax.rem(me + 2 * i, n)
            got_kv(source).wait_recv()
            share_kv(source).start()
            return 0

        lax.fori_loop(1, n // 2, pass_on, 0)
        own_q.wait()
        for d in order:
            got_q(lax.rem(head + d, heads)).wait_recv()

        def from_partner(i, _):
            got_kv(2 * i + 1 - core).wait_recv()
            return 0

        lax.fori_loop(0, n // 2, from_partner, 0)

    for p in range(pairs):
        for s in range(2):
            q = q_in[heads - 1 - 2 * p - s].astype(F32)
            qm[p, span * s : span * s + side] = jnp.where(lane_side < headed, q, 0.0).astype(BF16)
            qm[p, span * s + side : span * (s + 1)] = jnp.where(lane_side < headed, swap(q), 0.0).astype(BF16)
    later = jnp.where(iota((2 * span, 2 * span), 0) % span > iota((2 * span, 2 * span), 1), 1.0, 0.0)
    later = jnp.where(iota((2 * span, 2 * span), 1) >= span, 1.0, later).astype(BF16)
    row = iota((2 * span, span), 0)
    ahead = iota((2 * span, span), 1) - jnp.where(row < span, row, row - span - crew * span)

    def last_block(p):
        return crew * (heads - 1 - 2 * p) + member

    def attend(block, p, masked):
        z = lax.dot_general(qm[p], kv_in[block, 0:span], (((1,), (1,)), ((), ())), preferred_element_type=F32)
        z = z + kv_in[block, span : span + ROWS].astype(F32)[0:1]
        soft = jnp.log(1.0 + jnp.exp(-jnp.abs(z)))
        rest = jnp.minimum(-z, 0.0) - soft
        if masked:
            past = ahead < (last_block(p) - block) * span
            rest = jnp.where(past, rest, 0.0)
        top = rest.astype(BF16)
        bottom = (rest - top.astype(F32)).astype(BF16)
        sums = dot(jnp.concatenate([top, bottom], axis=1), later)
        power = jnp.exp(jnp.minimum(z, 0.0) - soft + (sums[:, 0:span] + carry[p]))
        if masked:
            power = jnp.where(past, power, 0.0)
        carry[p] += sums[:, span : 2 * span]
        acc[p] += dot(power.astype(BF16), kv_in[block, 0:span])

    def segment(s):
        def body(i, _):
            block = last_block(s) - i
            for p in range(s):
                attend(block, p, False)
            attend(block, s, True)
            return 0

        lax.fori_loop(0, 2 * crew if s < pairs - 1 else crew + member + 1, body, 0)

    for s in range(pairs):
        with scope(f"attend{s}"):
            segment(s)
        if s == max(pairs - 3, 0):
            with scope("wfwd"):
                for w in range(3):
                    for way in range(2):
                        arrived(w, way, way).wait_recv()
                        forward(w, way).start()

    def send_a(j):
        return along(a_out.at[j], a_in.at[head], a_send.at[j], a_recv.at[head], crew * j + member)

    def got_a(h):
        return along(a_out.at[h], a_in.at[h], a_send.at[h], a_recv.at[h], crew * h + member)

    with scope("asend"):
        for p in range(pairs):
            for s in range(2):
                a = acc[p, span * s : span * (s + 1)]
                a_out[heads - 1 - 2 * p - s] = jnp.where(lane_side < headed, swap(a[0:side]), a[side:span]).astype(BF16)
        own_a = pltpu.make_async_copy(a_out.at[head], a_in.at[head], loc_sem.at[9])
        own_a.start()
        for d in order:
            send_a(lax.rem(head + d, heads)).start()

    with scope("dwait"):
        each_peer(lambda peer: dispatched(peer).wait_recv())
        own_in.wait()

    xb[0:slots] = in_buf[:, 0:model]
    row8 = iota((ROWS, half), 0)

    def join(i, _):
        base = pl.multiple_of(i * 4 * ROWS, 4 * ROWS)
        four = in_buf[pl.ds(base, 4 * ROWS), model:wide].astype(F32)
        lefts, rights = [], []
        for j in range(2):
            even, odd = four[2 * ROWS * j : 2 * ROWS * j + ROWS], four[2 * ROWS * j + ROWS : 2 * ROWS * (j + 1)]
            lefts.append(jnp.where(row8 < 4, even, half_turn(odd)))
            rights.append(jnp.where(row8 < 4, half_turn(even), odd))
        to = pl.ds(pl.multiple_of(slots + i * 2 * ROWS, 2 * ROWS), 2 * ROWS)
        xb[to, 0:half] = jnp.concatenate(lefts, axis=0).astype(BF16)
        xb[to, half:model] = jnp.concatenate(rights, axis=0).astype(BF16)
        return 0

    lax.fori_loop(0, n // 4, join, 0)

    chunk = 512

    def serve(slot, number):
        rows = xb[...]
        g = dot(rows, gate[slot])
        u = dot(rows, up[slot])
        hidden = (g / (1.0 + jnp.exp(-g)) * u).astype(BF16)
        for c in range(model // chunk):
            at = slice(c * chunk, (c + 1) * chunk)
            term = dot(hidden, down[slot, :, at]).astype(BF16).astype(F32)
            if number == 0:
                total[:, at] = term
            else:
                total[:, at] += term

    with scope("serve3"):
        for c in local[0:3]:
            c.wait()
        serve(col, 0)
        for w in range(3):
            arrived(w, 0, 1).wait_recv()
        serve(left, 1)
        for w in range(3):
            arrived(w, 1, 0).wait_recv()
        serve(right, 2)
    with scope("farwait"):
        for w in range(3):
            forwarded(w, 0).wait_recv()
            forwarded(w, 1).wait_recv()
    with scope("serve1"):
        serve(far, 3)
        back[:, 0:model] = total[0:slots].astype(BF16)

        def part(i, _):
            at = pl.ds(pl.multiple_of(slots + i * ROWS, ROWS), ROWS)
            lefts, rights = total[at, 0:half], total[at, half:model]
            even = jnp.where(row8 < 4, lefts, half_turn(rights))
            odd = jnp.where(row8 < 4, half_turn(lefts), rights)
            to = pl.ds(pl.multiple_of(i * 2 * ROWS, 2 * ROWS), 2 * ROWS)
            back[to, model:wide] = jnp.concatenate([even, odd], axis=0).astype(BF16)
            return 0

        lax.fori_loop(0, n // 2, part, 0)
    each_peer(lambda peer: give_back(peer).start())
    own_back = pltpu.make_async_copy(strip(back, me), strip(ret, me), loc_sem.at[7])
    own_back.start()

    with scope("await"):
        own_a.wait()
        for d in order:
            got_a(lax.rem(head + d, heads)).wait_recv()
        local[3].wait()
    columns = []
    for p in range(pairs):
        a, b = a_in[2 * p].astype(F32), a_in[2 * p + 1].astype(F32)
        columns.append(
            jnp.concatenate(
                [jnp.where(lane_side < headed, a, swap(b)), jnp.where(lane_side < headed, swap(a), b)], axis=0
            )
        )
    attended = jnp.concatenate(columns, axis=1).astype(BF16)
    share = span // t
    proj[...] = dot(attended, ow[...]).astype(BF16)

    def shares(ref, index):
        return ref.at[pl.ds(pl.multiple_of(index * share, share), share)]

    def project(peer, slot):
        return pltpu.make_async_remote_copy(
            src_ref=shares(proj, peer), dst_ref=shares(proj_in, slot), send_sem=p_send.at[peer], recv_sem=p_recv.at[slot],
            device_id={"tp": peer}, device_id_type=MESH,
        )

    own_share = pltpu.make_async_copy(shares(proj, col), shares(proj_in, col), loc_sem.at[8])
    own_share.start()
    for d in range(1, t):
        project(lax.rem(col + d, t), col).start()
    own_share.wait()
    with scope("pwait"):
        for d in range(1, t):
            peer = lax.rem(col + d, t)
            project(peer, peer).wait_recv()
    projected = proj_in[0:share].astype(F32)
    for i in range(1, t):
        projected = projected + proj_in[i * share : (i + 1) * share].astype(F32)
    mixed_ref[...] = norm_rows(projected, mix_gain_ref[...]).astype(BF16)

    with scope("retwait"):
        each_peer(lambda peer: given_back(peer).wait_recv())
        own_back.wait()
    with scope("combine"):
        for c in range(2):
            at = slice(c * half, (c + 1) * half)
            tail = ret[:, model:wide]
            mix = dot(marks[0, 0], ret[:, at]) + dot(marks[0, 1], ret[:, at])
            mix = mix + dot(marks[1 + c, 0], tail) + dot(marks[1 + c, 1], tail)
            moe_ref[:, at] = mix.astype(BF16)

    for w in range(3):
        for way in range(2):
            forward(w, way).wait_send()
            for s in range(2):
                direct(w, way, s).wait_send()
    for d in order:
        h = lax.rem(head + d, heads)
        send_q(h).wait_send()
        send_a(h).wait_send()
        for c in range(chips):
            send_kv(h, c).wait_send()
    for c in range(1, chips):
        send_kv(head, lax.rem(chip + c, chips)).wait_send()

    def left_here(peer):
        dispatch(peer).wait_send()
        give_back(peer).wait_send()

    each_peer(left_here)

    def to_partner(i, _):
        share_kv(2 * i + core).wait_send()
        return 0

    lax.fori_loop(0, n // 2, to_partner, 0)
    for d in range(1, t):
        project(lax.rem(col + d, t), col).wait_send()


def per_device(
    queries, keys, values, stop_bias, out_weight, mix_gain, moe_input, ffn_gain, expert_ids, expert_scores,
    gate_weight, up_weight, down_weight,
):
    n, t = lax.axis_size("ep"), lax.axis_size("tp")
    span, width = queries.shape
    heads = stop_bias.shape[1]
    tokens, model = moe_input.shape
    hidden = gate_weight.shape[2]
    slots, wide, pairs, lanes = n * ROWS, model + model // 2, heads // 2, 2 * width // heads
    vmem, anywhere = pl.BlockSpec(memory_space=pltpu.VMEM), pl.BlockSpec(memory_space=pl.ANY)
    dma = pltpu.SemaphoreType.DMA
    return pl.pallas_call(
        functools.partial(kernel, n, t),
        out_shape=(
            jax.ShapeDtypeStruct((span // t, model), BF16),
            jax.ShapeDtypeStruct((tokens, model), BF16),
        ),
        in_specs=[
            vmem, vmem, vmem, vmem, anywhere, vmem, vmem, vmem, vmem, vmem, anywhere, anywhere, anywhere,
        ],
        out_specs=(vmem, vmem),
        scratch_shapes=[
            pltpu.VMEM((t, model, hidden), BF16),
            pltpu.VMEM((t, model, hidden), BF16),
            pltpu.VMEM((t, hidden, model), BF16),
            pltpu.VMEM(out_weight.shape, BF16),
            pltpu.VMEM((heads, span // 2, lanes), BF16),
            pltpu.VMEM((heads, span // 2, lanes), BF16),
            pltpu.VMEM((heads, span + ROWS, lanes), BF16),
            pltpu.VMEM((n, span + ROWS, lanes), BF16),
            pltpu.VMEM((heads, span // 2, lanes), BF16),
            pltpu.VMEM((heads, span // 2, lanes), BF16),
            pltpu.VMEM((pairs, 2 * span, lanes), BF16),
            pltpu.VMEM((pairs, 2 * span, lanes), F32),
            pltpu.VMEM((pairs, 2 * span, span), F32),
            pltpu.VMEM((slots, wide), BF16),
            pltpu.VMEM((slots, wide), BF16),
            pltpu.VMEM((slots, wide), BF16),
            pltpu.VMEM((slots, wide), BF16),
            pltpu.VMEM((slots + slots // 2, model), BF16),
            pltpu.VMEM((slots + slots // 2, model), F32),
            pltpu.VMEM((3, 2, tokens, slots), BF16),
            pltpu.VMEM((span, model), BF16),
            pltpu.VMEM((span, model), BF16),
            dma((10,)),
            dma((2, 3, 2)),
            dma((2, 3, 2)),
            dma((2, 3)),
            dma((2, 3)),
            dma((heads,)),
            dma((heads,)),
            dma((heads, n // heads // 2)),
            dma((n,)),
            dma((n,)),
            dma((heads,)),
            dma((heads,)),
            dma((n,)),
            dma((n,)),
            dma((n,)),
            dma((n,)),
            dma((t,)),
            dma((t,)),
        ],
        compiler_params=pltpu.CompilerParams(
            collective_id=0, has_side_effects=True, vmem_limit_bytes=60 * 1024 * 1024
        ),
    )(
        queries, keys, values, stop_bias.T, out_weight, mix_gain[None, :], moe_input, ffn_gain[None, :],
        expert_ids.T, expert_scores.T, gate_weight, up_weight, down_weight,
    )


def solution(mesh):
    placed = (
        P(GRP_EP, "tp"), P(GRP_EP, "tp"), P(GRP_EP, "tp"), P(GRP_EP, "tp"), P("tp", None), P(), P(GRP_EP_TP, None), P(),
        P(GRP_EP_TP, None), P(GRP_EP_TP, None), P("ep", None, "tp"), P("ep", None, "tp"), P("ep", "tp", None),
    )
    return jax.shard_map(
        per_device,
        mesh=mesh,
        in_specs=placed,
        out_specs=(P(GRP_EP_TP, None), P(GRP_EP_TP, None)),
        check_vma=False,
    )
```

time: 268 us -> 217 us (0.81)
  the two profiles are of different devices: /device:TPU:1953 before, /device:TPU:33 now
where the time goes in v2:
time: 217 us
  Pallas kernels  213 us (98%)
  local copies, waits for them, and re-layouts  3.45 us (2%)
    pallas_call x1, Pallas kernels, per_device(): pl.pallas_call(functools.partial(kernel, n, t), out_shape=(jax.ShapeDtype...  213 us

profile of v2, /device:TPU:33, one launch (start us, length us, event | category | flops | bytes accessed | tf_op | source)
XLA Modules:
  0.0 217.0 jit_solution(13498847967313855193)
XLA Ops:
  0.6 212.9 %shard_map.140 = (bf16[32,2048]{1,0:T(8,128)(2,1)}, bf16[128,2048]{1,0:T(8,128)(2,1)}) custom-call(bf16[128,512]{1,0:T(8,128)(2,1)} %q_ref.1, bf16[128,512]{1,0:T(8,128)(2,1)} %k_ref.1, bf16[128,512]{1,0:T(8,128)(2,1)} %v_ref.1, bf16[8,128]{1,0:T(8,128)(2,1)} %bitcast.7, bf16[512,2048]{1,0:T(8,128)(2,1)} %ow_ref.1, f32[1,2048]{1,0:T(1,128)} %bitcast.5, ...), custom_call_target="tpu_custom_call" | custom-call | tf_op jit(solution)/shard_map/pallas_call | solution.py:480
  213.5 1.6 copy.17
  215.1 1.9 copy.18
